TPU v7x, 32 devices: a whole 2x2x4 slice. The times are simulated.
32 devices in a mesh: ep: 8 (over z, x), tp: 4 (over y, core).
Axes of the slice: x: 2, y: 2, z: 4, core: 2. Of those that a mesh axis runs over, the one named last changes fastest.
Arguments:
- hidden_in: bfloat16 [128, 4096], P('ep'), may hold values from -6 to 6
- w_query: bfloat16 [4096, 2048], P('ep', 'tp'), may hold values from -0.09375 to 0.09375
- w_key: bfloat16 [4096, 2048], P('ep', 'tp'), may hold values from -0.09375 to 0.09375
- w_value: bfloat16 [4096, 2048], P('ep', 'tp'), may hold values from -0.09375 to 0.09375
- w_outgate: bfloat16 [4096, 2048], P('ep', 'tp'), may hold values from -0.09375 to 0.09375
- w_igate: bfloat16 [4096, 16], P('ep', 'tp'), may hold values from -0.09375 to 0.09375
- w_fgate: bfloat16 [4096, 16], P('ep', 'tp'), may hold values from -0.09375 to 0.09375
- input_bias: float32 [16], P('tp'), may hold values from -3 to 303
- forget_bias: float32 [16], P('tp'), may hold values from -1 to 5
- mem_state: float32 [128, 16, 16384], P('ep', 'tp'), may hold values from -4 to 4
- max_state: float32 [128, 16], P('ep', 'tp'), may hold values from -4 to 304
- head_gain: float32 [2048], P('tp'), may hold values from 0.1 to 1.9
- w_output: bfloat16 [2048, 4096], P('tp'), may hold values from -0.26367188 to 0.26367188
- first_gain: float32 [4096], replicated, may hold values from 0.35 to 3.25
- w_group_router: bfloat16 [4096, 2], replicated, may hold values from -0.09375 to 0.09375
- w_expert_router: bfloat16 [4096, 8], replicated, may hold values from -0.09375 to 0.09375
- expert_route: int32 [128, 2], P('ep'), may hold values from 0 to 7, as said below
- w_expgate: bfloat16 [8, 4096, 1024], P('ep', None, 'tp'), may hold values from -0.09375 to 0.09375
- w_expup: bfloat16 [8, 4096, 1024], P('ep', None, 'tp'), may hold values from -0.09375 to 0.09375
- w_expdown: bfloat16 [8, 1024, 4096], P('ep', 'tp'), may hold values from -0.75 to 0.75
- second_gain: float32 [4096], P('tp'), may hold values from 0.1 to 1.9
Outputs:
- hidden_out: bfloat16 [128, 4096], P('ep', 'tp')
- mem_next: float32 [128, 16, 16384], P('ep', 'tp')
- max_next: float32 [128, 16], P('ep', 'tp')
Inputs may be any that keep to these rules, and one draw needn't show every extreme that they name: `expert_route`: each row names two different experts of one group (an expert's group is its number divided by 4). In each aligned block of 16 rows (the rows of one index of ep) every group is named by exactly 8 rows, no expert by more than 8 rows, and some expert by exactly 8 rows.
All inputs are finite; a program needn't handle non-finite values.
Results may differ from a plain program's by a relative error of at most 0.02.
Values may be sent and summed in bfloat16 or wider, within the bound.
A program may use at most 64 MiB of HBM per device.

v0:
```python
import jax
import jax.numpy as jnp
from jax import lax
from jax.sharding import PartitionSpec as P

D = 4096
DH = 128
GROUP_SIZE = 4
res_alpha = 8.0**0.25


def layer_norm(values, gain):
    row_mean = jnp.mean(values, -1, keepdims=True)
    row_var = jnp.mean(values * values, -1, keepdims=True) - row_mean * row_mean
    return (values - row_mean) * lax.rsqrt(row_var + 1e-05) * gain


def mlstm_step(queries, keys_scaled, values, log_input, log_forget, memory, stabilizer):
    new_max = jnp.maximum(log_forget + stabilizer, log_input)
    keep_old = jnp.exp(log_forget + stabilizer - new_max)
    write_new = jnp.exp(log_input - new_max)
    scores = jnp.sum(queries * keys_scaled, -1) * write_new
    read_old = jnp.einsum("bhd,bhde->bhe", queries, memory, precision=lax.Precision.HIGHEST)
    readout = scores[..., None] * values + keep_old[..., None] * read_old
    memory_next = (
        keep_old[..., None, None] * memory
        + write_new[..., None, None] * keys_scaled[..., :, None] * values[..., None, :]
    )
    return (readout, memory_next, new_max)


def head_mix(readout, head_gain, out_pre):
    scaled = readout * lax.rsqrt(jnp.mean(readout * readout, -1, keepdims=True) + 1e-06)
    flat_heads = scaled.reshape(scaled.shape[0], -1)
    return (flat_heads * head_gain * jax.nn.sigmoid(out_pre)).astype(jnp.bfloat16)


def route_weights(mid_float, w_group_router, w_expert_router, expert_route):
    group_logits = jnp.dot(
        mid_float, w_group_router.astype(jnp.float32), precision=lax.Precision.HIGHEST
    )
    expert_logits = jnp.dot(
        mid_float, w_expert_router.astype(jnp.float32), precision=lax.Precision.HIGHEST
    )
    first_expert = expert_route[:, 0]
    second_expert = expert_route[:, 1]
    expert_ids = lax.broadcasted_iota(jnp.int32, expert_logits.shape, 1)
    group_ids = lax.broadcasted_iota(jnp.int32, group_logits.shape, 1)
    first_logit = jnp.sum(jnp.where(expert_ids == first_expert[:, None], expert_logits, 0.0), -1)
    second_logit = jnp.sum(jnp.where(expert_ids == second_expert[:, None], expert_logits, 0.0), -1)
    group_pick = jnp.sum(
        jnp.where(group_ids == (first_expert // GROUP_SIZE)[:, None], group_logits, 0.0), -1
    )
    group_gate = jax.nn.sigmoid(group_pick)
    return (
        group_gate * jax.nn.sigmoid(first_logit - second_logit),
        group_gate * jax.nn.sigmoid(second_logit - first_logit),
    )


def slot_ranks(flat_routes, expert_total):
    onehot = (
        flat_routes[:, None]
        == lax.broadcasted_iota(jnp.int32, (flat_routes.shape[0], expert_total), 1)
    ).astype(jnp.int32)
    running = jnp.cumsum(onehot, 0)
    return jnp.sum((running - 1) * onehot, -1)


def body(
    hidden_in,
    w_query,
    w_key,
    w_value,
    w_outgate,
    w_igate,
    w_fgate,
    input_bias,
    forget_bias,
    mem_state,
    max_state,
    head_gain,
    w_output,
    first_gain,
    w_group_router,
    w_expert_router,
    expert_route,
    w_expgate,
    w_expup,
    w_expdown,
    second_gain,
):
    own_rows, width = hidden_in.shape
    heads_here = mem_state.shape[1]
    head_width = heads_here * DH
    top_count = expert_route.shape[1]
    spread_rows = lax.all_to_all(hidden_in, "ep", split_axis=1, concat_axis=0, tiled=True)
    stacked_w = jnp.concatenate([w_query, w_key, w_value, w_outgate], 1)
    gate_w = jnp.concatenate([w_igate, w_fgate], 1)
    proj_terms = jnp.dot(spread_rows, stacked_w, preferred_element_type=jnp.float32)
    gate_terms = jnp.dot(spread_rows, gate_w, preferred_element_type=jnp.float32)
    projected, gate_sums = (
        lax.psum_scatter(proj_terms, "ep", scatter_dimension=0, tiled=True),
        lax.psum_scatter(gate_terms, "ep", scatter_dimension=0, tiled=True),
    )
    shaped = projected.reshape(own_rows, 4, heads_here, DH)
    queries = shaped[:, 0]
    keys_raw = shaped[:, 1]
    values = shaped[:, 2]
    out_pre = shaped[:, 3].reshape(own_rows, head_width)
    input_sum = gate_sums[:, :heads_here]
    forget_sum = gate_sums[:, heads_here:]
    keys_scaled = keys_raw * DH ** (-0.5)
    log_input = input_sum + input_bias
    log_forget = jax.nn.log_sigmoid(forget_sum + forget_bias)
    memory = mem_state.reshape(own_rows, heads_here, DH, DH)
    readout, memory_square, new_max = mlstm_step(
        queries, keys_scaled, values, log_input, log_forget, memory, max_state
    )
    memory_next = memory_square.reshape(own_rows, heads_here, DH * DH)
    mixed_heads = head_mix(readout, head_gain, out_pre)
    partial_mix = jnp.dot(mixed_heads, w_output, preferred_element_type=jnp.float32).astype(
        jnp.bfloat16
    )
    mix = lax.psum(partial_mix.astype(jnp.float32).astype(jnp.bfloat16), "tp").astype(jnp.float32)
    mid_float = layer_norm(res_alpha * hidden_in.astype(jnp.float32) + mix, first_gain)
    mid = mid_float.astype(jnp.bfloat16)
    first_weight, second_weight = route_weights(
        mid_float, w_group_router, w_expert_router, expert_route
    )
    expert_total = w_expgate.shape[0] * lax.axis_size("ep")
    capacity = 2 * own_rows * top_count // expert_total
    flat_routes = expert_route.reshape(-1)
    local_slot = flat_routes * capacity + slot_ranks(flat_routes, expert_total)
    share_width = width // lax.axis_size("tp")
    mid_share = lax.dynamic_slice_in_dim(mid, lax.axis_index("tp") * share_width, share_width, 1)
    buffer = (
        jnp.zeros((expert_total * capacity, width), jnp.bfloat16)
        .at[local_slot]
        .set(jnp.repeat(mid, top_count, 0))
    )
    arrived = lax.all_to_all(
        buffer.reshape(expert_total, capacity, width), "ep", split_axis=0, concat_axis=1, tiled=True
    )
    gate_pre = jnp.einsum("erd,edf->erf", arrived, w_expgate, preferred_element_type=jnp.float32)
    up_pre = jnp.einsum("erd,edf->erf", arrived, w_expup, preferred_element_type=jnp.float32)
    hidden_units = (jax.nn.silu(gate_pre) * up_pre).astype(jnp.bfloat16)
    down_terms = jnp.einsum(
        "erf,efd->erd", hidden_units, w_expdown, preferred_element_type=jnp.float32
    ).astype(jnp.bfloat16)
    expert_share = lax.psum_scatter(
        down_terms.astype(jnp.float32).astype(jnp.bfloat16), "tp", scatter_dimension=2, tiled=True
    )
    returned = lax.all_to_all(expert_share, "ep", split_axis=1, concat_axis=0, tiled=True)
    picked = returned.reshape(expert_total * capacity, share_width)[local_slot]
    picked = picked.astype(jnp.float32).reshape(own_rows, top_count, share_width)
    moe = first_weight[:, None] * picked[:, 0] + second_weight[:, None] * picked[:, 1]
    joined = res_alpha * mid_share.astype(jnp.float32) + moe
    row_sum, square_sum = lax.psum((jnp.sum(joined, -1), jnp.sum(joined * joined, -1)), "tp")
    row_mean = row_sum / D
    row_var = square_sum / D - row_mean * row_mean
    hidden_out = (
        (joined - row_mean[:, None]) * lax.rsqrt(row_var[:, None] + 1e-05) * second_gain
    ).astype(jnp.bfloat16)
    return (hidden_out, memory_next, new_max)


def solution(mesh):
    return jax.shard_map(
        body,
        mesh=mesh,
        in_specs=(
            P("ep", None),
            P("ep", "tp"),
            P("ep", "tp"),
            P("ep", "tp"),
            P("ep", "tp"),
            P("ep", "tp"),
            P("ep", "tp"),
            P("tp"),
            P("tp"),
            P("ep", "tp", None),
            P("ep", "tp"),
            P("tp"),
            P("tp", None),
            P(),
            P(),
            P(),
            P("ep", None),
            P("ep", None, "tp"),
            P("ep", None, "tp"),
            P("ep", "tp", None),
            P("tp"),
        ),
        out_specs=(P("ep", "tp"), P("ep", "tp", None), P("ep", "tp")),
        check_vma=False,
    )
```

profile of v0, /device:TPU:0, one launch (start us, length us, event | category | flops | bytes accessed | tf_op | source)
XLA Modules:
  0.0 277.9 jit_solution(14590576950777728029)
XLA Ops:
  8.3 14.4 %all_to_all.37 = bf16[16,8,512]{2,0,1:T(8,128)(2,1)S(1)} all-to-all(bf16[16,8,512]{2,0,1:T(8,128)(2,1)S(1)} %bitcast.124), channel_id=1, replica_groups=mesh['ep'=8,'tp'=4] {'ep'}, dimensions={1} | all-to-all | bytes 262144 | tf_op jit(solution)/shard_map/all_to_all | solution.py:97
  24.4 2.3 convolution_bitcast_fusion
  26.6 1.3 copy.104
  28.1 6.1 %reshape.183 = f32[16,4,128,128]{3,2,1,0:T(8,128)} reshape(f32[16,4,16384]{2,1,0:T(4,128)} %param.30) | data formatting | bytes 8388608 | tf_op jit(solution)/shard_map/reshape | solution.py:116
  34.9 49.9 %reduce-scatter.12.cloned.1.call-done = f32[16,8]{1,0:T(8,128)} async-done(((f32[128,8]{1,0:T(8,128)}), f32[16,8]{1,0:T(8,128)}) %reduce-scatter.12.cloned.1.call-update) | async-done | bytes 528 | tf_op jit(solution)/shard_map/reduce_scatter | solution.py:104
  85.7 66.2 %reduce-scatter.10.cloned.1.call-done = f32[16,2048]{1,0:T(8,128)} async-done(((f32[128,2048]{1,0:T(8,128)}), f32[16,2048]{1,0:T(8,128)}) %reduce-scatter.10.cloned.1.call-update) | async-done | bytes 131088
  151.8 1.2 copy.105
  157.3 5.3 %fusion.64 = f32[16,4,1,128]{3,2,1,0:T(1,128)S(1)} fusion(f32[16,4,128,1]{2,3,1,0:T(1,128)S(1)} %bitcast.125, f32[16,4,128,128]{3,2,1,0:T(8,128)} %reshape.183), kind=kOutput, calls=%fused_computation.111 | convolution fusion | flops 12582912 | bytes 4259840 | tf_op jit(solution)/shard_map/bhd,bhde->bhe/dot_general | solution.py:23
  163.3 3.5 %convolution_convert_fusion.1 = bf16[16,4096]{1,0:T(8,128)(2,1)} fusion(bf16[512,4096]{1,0:T(8,128)(2,1)} %param.33, f32[2,8,4,128]{3,2,1,0:T(4,128)S(1)} %bitcast.128, f32[2,8,4,128]{3,2,1,0:T(4,128)S(1)} %bitcast.129, f32[512]{0:T(512)S(1)} %copy-done.7), kind=kOutput, calls=%fused_computation.4 | convolution fusion | flops 67198976 | bytes 4392960 | tf_op jit(solution)/shard_map/dot_general | solution.py:122
  166.8 30.9 %all-reduce.3.cloned.1.call-done = bf16[16,4096]{1,0:T(8,128)(2,1)} async-done(((bf16[16,4096]{1,0:T(8,128)(2,1)}), bf16[16,4096]{1,0:T(8,128)(2,1)}) %all-reduce.3.cloned.1.call-update) | async-done | bytes 131088 | tf_op jit(solution)/shard_map/psum | solution.py:125
  200.1 1.8 scatter_custom_fusion
  201.9 5.5 %all-to-all-start.1 = ((bf16[8,8,4096]{2,1,0:T(8,128)(2,1)}), bf16[8,8,4096]{2,1,0:T(8,128)(2,1)S(1)}, u32[]{:S(2)}, u32[]{:S(2)}) async-start(bf16[8,8,4096]{2,1,0:T(8,128)(2,1)} %bitcast.18), calls=%async_computation.1 | async-start | bytes 1048576 | tf_op jit(solution)/shard_map/all_to_all | solution.py:142
  208.1 2.6 broadcast_multiply_fusion
  210.8 5.6 %mul.268 = f32[16,4,16384]{2,1,0:T(4,128)} reshape(f32[16,4,128,128]{3,2,1,0:T(8,128)} %broadcast_multiply_fusion) | data formatting | bytes 8388608 | tf_op jit(solution)/shard_map/mul | solution.py:27
  216.3 4.5 %all-to-all-done.1 = bf16[8,8,4096]{2,1,0:T(8,128)(2,1)S(1)} async-done(((bf16[8,8,4096]{2,1,0:T(8,128)(2,1)}), bf16[8,8,4096]{2,1,0:T(8,128)(2,1)S(1)}, u32[]{:S(2)}, u32[]{:S(2)}) %all-to-all-start.1) | async-done | bytes 524320 | tf_op jit(solution)/shard_map/all_to_all | solution.py:142
  220.8 2.0 fusion.11
  222.9 3.8 %fusion = bf16[1,64,4096]{2,1,0:T(8,128)(2,1)} fusion(bf16[1,256,4096]{2,1,0:T(8,128)(2,1)S(1)} %copy-done, bf16[1,4096,256]{2,1,0:T(8,128)(2,1)} %param.39, bf16[8,8,4096]{2,1,0:T(8,128)(2,1)S(1)} %all-to-all-done.1, f32[64,256]{1,0:T(8,128)S(1)} %fusion.11), kind=kOutput, calls=%fused_computation.3 | convolution fusion | flops 268795904 | bytes 5308416 | tf_op jit(solution)/shard_map/erf,efd->erd/dot_general | solution.py:148
  226.7 6.9 %multiply_add_fusion = f32[16,4,16384]{2,1,0:T(4,128)} fusion(f32[16,4,16384]{2,1,0:T(4,128)} %mul.268, f32[16,4,16384]{2,1,0:T(4,128)} %param.30, f32[16,4]{1,0:T(8,128)S(1)} %get-tuple-element.28), kind=kLoop, calls=%fused_computation.5 | loop fusion | flops 2097152 | bytes 12583168 | tf_op jit(solution)/shard_map/add | solution.py:26
  234.4 12.5 %reduce-scatter.8.cloned.1.call-done = bf16[1,64,1024]{2,1,0:T(8,128)(2,1)} async-done(((bf16[1,64,4096]{2,1,0:T(8,128)(2,1)}), bf16[1,64,1024]{2,1,0:T(8,128)(2,1)}) %reduce-scatter.8.cloned.1.call-update) | async-done | bytes 131088 | tf_op jit(solution)/shard_map/reduce_scatter | solution.py:151
  246.9 1.1 copy.141
  248.5 1.4 reduce
  250.6 5.5 %all-to-all-start.2 = ((bf16[8,2,4096]{2,1,0:T(2,128)(2,1)}), bf16[8,2,4096]{2,1,0:T(2,128)(2,1)S(1)}, u32[]{:S(2)}, u32[]{:S(2)}) async-start(bf16[8,2,4096]{2,1,0:T(2,128)(2,1)} %reshape.217), calls=%async_computation.3 | async-start | bytes 262144 | tf_op jit(solution)/shard_map/all_to_all | solution.py:154
  256.2 7.3 %all-to-all-done.2 = bf16[8,2,4096]{2,1,0:T(2,128)(2,1)S(1)} async-done(((bf16[8,2,4096]{2,1,0:T(2,128)(2,1)}), bf16[8,2,4096]{2,1,0:T(2,128)(2,1)S(1)}, u32[]{:S(2)}, u32[]{:S(2)}) %all-to-all-start.2) | async-done | bytes 131104 | tf_op jit(solution)/shard_map/all_to_all | solution.py:154
  264.7 5.9 %all-reduce = (f32[16]{0:T(128)S(1)}, f32[16]{0:T(128)S(1)}) all-reduce(f32[16]{0:T(128)S(1)} %get-tuple-element.9, f32[16]{0:T(128)S(1)} %get-tuple-element.8), channel_id=1, replica_groups=mesh['ep'=8,'tp'=4] {'tp'}, use_global_device_ids=true, to_apply=%region_17.18 | all-reduce | flops 32 | bytes 256 | tf_op jit(solution)/shard_map/psum | solution.py:159
  (82 shorter events, 16.2 us)
Async XLA Ops:
  7.2 215.7 %copy-start = (bf16[1,256,4096]{2,1,0:T(8,128)(2,1)S(1)}, bf16[1,256,4096]{2,1,0:T(8,128)(2,1)}, u32[]{:S(2)}) copy-start(bf16[1,256,4096]{2,1,0:T(8,128)(2,1)} %param.40) | copy-start | bytes 6291460
  7.2 77.6 %reduce-scatter.12.cloned.1.call-start = ((), (), s32[]{:S(2)}) async-start(), calls=%async_computation.9 | async-start | bytes 73728 | tf_op jit(solution)/shard_map/reduce_scatter | solution.py:104
  24.3 3.7 %copy-start.10 = (f32[16,4]{0,1:T(4,128)S(1)}, f32[16,4]{0,1:T(4,128)}, u32[]{:S(2)}) copy-start(f32[16,4]{0,1:T(4,128)} %param.31) | copy-start | bytes 772
  24.3 127.5 %reduce-scatter.10.cloned.1.call-start = ((), (), s32[]{:S(2)}) async-start(), calls=%async_computation.8 | async-start | bytes 1179648
  28.0 169.7 %all-reduce.3.cloned.1.call-start = ((), (), s32[]{:S(2)}) async-start(), calls=%async_computation.6 | async-start | bytes 262144 | tf_op jit(solution)/shard_map/psum | solution.py:125
  28.1 6.1 %copy-start.5 = (s32[16,2]{0,1:T(2,128)S(1)}, s32[16,2]{0,1:T(2,128)}, u32[]{:S(2)}) copy-start(s32[16,2]{0,1:T(2,128)} %param.37) | copy-start | bytes 388
  28.1 56.7 %copy-start.8 = (f32[4]{0:T(128)S(1)}, f32[4]{0:T(128)}, u32[]{:S(2)}) copy-start(f32[4]{0:T(128)} %param.28) | copy-start | bytes 52
  28.1 56.7 %copy-start.9 = (f32[4]{0:T(128)S(1)}, f32[4]{0:T(128)}, u32[]{:S(2)}) copy-start(f32[4]{0:T(128)} %param.29) | copy-start | bytes 52
  85.7 77.0 %copy-start.3 = (f32[16,8]{1,0:T(8,128)S(1)}, f32[16,8]{1,0:T(8,128)}, u32[]{:S(2)}) copy-start(f32[16,8]{1,0:T(8,128)} %reduce-scatter.12.cloned.1.call-done) | copy-start | bytes 1540
  153.1 10.2 %copy-start.7 = (f32[512]{0:T(512)S(1)}, f32[512]{0:T(512)}, u32[]{:S(2)}) copy-start(f32[512]{0:T(512)} %param.32) | copy-start | bytes 6148
  157.3 40.4 %copy-start.1 = (bf16[16,4096]{1,0:T(8,128)(2,1)S(1)}, bf16[16,4096]{1,0:T(8,128)(2,1)}, u32[]{:S(2)}) copy-start(bf16[16,4096]{1,0:T(8,128)(2,1)} %param.21) | copy-start | bytes 393220
  157.3 41.5 %copy-start.4 = (f32[4096]{0:T(1024)S(1)}, f32[4096]{0:T(1024)}, u32[]{:S(2)}) copy-start(f32[4096]{0:T(1024)} %param.34) | copy-start | bytes 49156
  201.9 18.9 %all-to-all-start.1 = ((bf16[8,8,4096]{2,1,0:T(8,128)(2,1)}), bf16[8,8,4096]{2,1,0:T(8,128)(2,1)S(1)}, u32[]{:S(2)}, u32[]{:S(2)}) async-start(bf16[8,8,4096]{2,1,0:T(8,128)(2,1)} %bitcast.18), calls=%async_computation.1 | async-start | bytes 1048576 | tf_op jit(solution)/shard_map/all_to_all | solution.py:142
  207.4 39.5 %reduce-scatter.8.cloned.1.call-start = ((), (), s32[]{:S(2)}) async-start(), calls=%async_computation.7 | async-start | bytes 655360 | tf_op jit(solution)/shard_map/reduce_scatter | solution.py:151
  226.7 6.9 %copy-start.2 = (bf16[16,4096]{1,0:T(8,128)(2,1)S(1)}, bf16[16,4096]{1,0:T(8,128)(2,1)}, u32[]{:S(2)}) copy-start(bf16[16,4096]{1,0:T(8,128)(2,1)} %all-reduce.3.cloned.1.call-done) | copy-start | bytes 393220
  226.7 6.9 %copy-start.12 = (bf16[4096,2]{0,1:T(2,128)(2,1)S(1)}, bf16[4096,2]{0,1:T(2,128)(2,1)}, u32[]{:S(2)}) copy-start(bf16[4096,2]{0,1:T(2,128)(2,1)} %param.35) | copy-start | bytes 49156
  226.7 7.3 %copy-start.11 = (bf16[4096,8]{0,1:T(8,128)(2,1)S(1)}, bf16[4096,8]{0,1:T(8,128)(2,1)}, u32[]{:S(2)}) copy-start(bf16[4096,8]{0,1:T(8,128)(2,1)} %param.36) | copy-start | bytes 196612
  233.6 37.1 %copy-start.6 = (f32[1024]{0:T(1024)S(1)}, f32[1024]{0:T(1024)}, u32[]{:S(2)}) copy-start(f32[1024]{0:T(1024)} %param.41) | copy-start | bytes 12292
  250.6 12.9 %all-to-all-start.2 = ((bf16[8,2,4096]{2,1,0:T(2,128)(2,1)}), bf16[8,2,4096]{2,1,0:T(2,128)(2,1)S(1)}, u32[]{:S(2)}, u32[]{:S(2)}) async-start(bf16[8,2,4096]{2,1,0:T(2,128)(2,1)} %reshape.217), calls=%async_computation.3 | async-start | bytes 262144 | tf_op jit(solution)/shard_map/all_to_all | solution.py:154
Sparse Core Ops, SparseCore 0:
  24.4 60.3 reduce-scatter.11
  88.2 63.5 reduce-scatter.9
  166.9 30.7 all-reduce.2
  226.8 20.0 reduce-scatter.7
where the time goes:
time: 279 us; the launch traced here: 278 us
  waiting for transfers between devices  171 us (61%)
  local copies, waits for them, and re-layouts  26.8 us (10%)
  blocking collectives  20.3 us (7%)
  matrix products  18.5 us (7%)
  other arithmetic  15.7 us (6%)
  between operations  14.1 us (5%)
  starting transfers between devices  11.2 us (4%)
    unnamed x5, waiting for transfers between devices  66.2 us
    reduce_scatter x1, waiting for transfers between devices, body(): lax.psum_scatter(gate_terms, 'ep', scatter_dimension=0, tiled=True)  49.9 us
    psum x1, waiting for transfers between devices, body(): lax.psum(partial_mix.astype(jnp.float32).astype(jnp.bfloat16), 'tp')  30.9 us
    all_to_all x1, blocking collectives, body(): lax.all_to_all(hidden_in, 'ep', split_axis=1, concat_axis=0, tiled=True)  14.4 us
    reduce_scatter x1, waiting for transfers between devices, body(): lax.psum_scatter(down_terms.astype(jnp.float32).astype(jnp.bfloat16), 'tp...  12.5 us
    unnamed x40, local copies, waits for them, and re-layouts  8.86 us
    all_to_all x1, waiting for transfers between devices, body(): lax.all_to_all(expert_share, 'ep', split_axis=1, concat_axis=0, tiled=True)  7.32 us
    add x1, other arithmetic, mlstm_step(): keep_old[..., None, None] * memory  6.88 us
  transfers between devices with their start and end apart: 6, of which 6 were waited for; matrix products, arithmetic and copies ran while one was open for 10% of the time, Pallas kernels for 0%

commit v1 on v0

--- a/solution.py
+++ b/solution.py
@@ -122,7 +122,9 @@
     partial_mix = jnp.dot(mixed_heads, w_output, preferred_element_type=jnp.float32).astype(
         jnp.bfloat16
     )
-    mix = lax.psum(partial_mix.astype(jnp.float32).astype(jnp.bfloat16), "tp").astype(jnp.float32)
+    mix = jnp.sum(
+        lax.all_gather(partial_mix.astype(jnp.float32).astype(jnp.bfloat16), "tp"), axis=0
+    ).astype(jnp.float32)
     mid_float = layer_norm(res_alpha * hidden_in.astype(jnp.float32) + mix, first_gain)
     mid = mid_float.astype(jnp.bfloat16)
     first_weight, second_weight = route_weights(

time: 279 us -> 252 us (0.903)
  waiting for transfers between devices: 171 us -> 142 us
  blocking collectives: 20.3 us -> 27.5 us
    psum x1 -> x0, waiting for transfers between devices: 30.9 us -> none  [body(): lax.psum(partial_mix.astype(jnp.float32).astype(jnp.bfloat16), 'tp')]
    all_gather x0 -> x1, blocking collectives: none -> 7.14 us  [body(): lax.all_gather(partial_mix.astype(jnp.float32).astype(jnp.bfloat16), 'tp')]
    unnamed x5 -> x4, waiting for transfers between devices: 66.2 us -> 66.2 us
    unnamed x40 -> x38, local copies, waits for them, and re-layouts: 8.86 us -> 8.85 us
  transfers between devices with their start and end apart: 6 -> 5, of which waited for: 6 -> 5; matrix products, arithmetic and copies ran while one was open for 10% -> 11% of each run, Pallas kernels for 0% -> 0%
where the time goes in v1:
time: 252 us; the launch traced here: 251 us
  waiting for transfers between devices  142 us (56%)
  blocking collectives  27.5 us (11%)
  local copies, waits for them, and re-layouts  26.8 us (11%)
  matrix products  17.8 us (7%)
  between operations  14.1 us (6%)
  other arithmetic  13.9 us (6%)
  starting transfers between devices  9.37 us (4%)
    unnamed x4, waiting for transfers between devices  66.2 us
    reduce_scatter x1, waiting for transfers between devices, body(): lax.psum_scatter(gate_terms, 'ep', scatter_dimension=0, tiled=True)  49.9 us
    all_to_all x1, blocking collectives, body(): lax.all_to_all(hidden_in, 'ep', split_axis=1, concat_axis=0, tiled=True)  14.4 us
    reduce_scatter x1, waiting for transfers between devices, body(): lax.psum_scatter(down_terms.astype(jnp.float32).astype(jnp.bfloat16), 'tp...  12.5 us
    unnamed x38, local copies, waits for them, and re-layouts  8.85 us
    all_to_all x1, waiting for transfers between devices, body(): lax.all_to_all(expert_share, 'ep', split_axis=1, concat_axis=0, tiled=True)  7.32 us
    all_gather x1, blocking collectives, body(): lax.all_gather(partial_mix.astype(jnp.float32).astype(jnp.bfloat16), 'tp')  7.14 us
    add x1, other arithmetic, mlstm_step(): keep_old[..., None, None] * memory  6.86 us
  transfers between devices with their start and end apart: 5, of which 5 were waited for; matrix products, arithmetic and copies ran while one was open for 11% of the time, Pallas kernels for 0%

profile of v1, /device:TPU:0, one launch (start us, length us, event | category | flops | bytes accessed | tf_op | source)
XLA Modules:
  0.0 251.4 jit_solution(14353363218824865677)
XLA Ops:
  8.3 14.4 %all_to_all.37 = bf16[16,8,512]{2,0,1:T(8,128)(2,1)S(1)} all-to-all(bf16[16,8,512]{2,0,1:T(8,128)(2,1)S(1)} %bitcast.126), channel_id=1, replica_groups=mesh['ep'=8,'tp'=4] {'ep'}, dimensions={1} | all-to-all | bytes 262144 | tf_op jit(solution)/shard_map/all_to_all | solution.py:97
  24.4 2.3 convolution_bitcast_fusion
  26.6 1.3 copy.106
  28.1 6.1 %reshape.183 = f32[16,4,128,128]{3,2,1,0:T(8,128)} reshape(f32[16,4,16384]{2,1,0:T(4,128)} %param.30) | data formatting | bytes 8388608 | tf_op jit(solution)/shard_map/reshape | solution.py:116
  34.9 49.9 %reduce-scatter.12.cloned.1.call-done = f32[16,8]{1,0:T(8,128)} async-done(((f32[128,8]{1,0:T(8,128)}), f32[16,8]{1,0:T(8,128)}) %reduce-scatter.12.cloned.1.call-update) | async-done | bytes 528 | tf_op jit(solution)/shard_map/reduce_scatter | solution.py:104
  85.7 66.2 %reduce-scatter.10.cloned.1.call-done = f32[16,2048]{1,0:T(8,128)} async-done(((f32[128,2048]{1,0:T(8,128)}), f32[16,2048]{1,0:T(8,128)}) %reduce-scatter.10.cloned.1.call-update) | async-done | bytes 131088
  151.8 1.2 copy.107
  157.3 5.3 %fusion.64 = f32[16,4,1,128]{3,2,1,0:T(1,128)S(1)} fusion(f32[16,4,128,1]{2,3,1,0:T(1,128)S(1)} %bitcast.127, f32[16,4,128,128]{3,2,1,0:T(8,128)} %reshape.183), kind=kOutput, calls=%fused_computation.111 | convolution fusion | flops 12582912 | bytes 4259840 | tf_op jit(solution)/shard_map/bhd,bhde->bhe/dot_general | solution.py:23
  163.2 2.8 %convolution_convert_fusion.1 = bf16[16,4096]{1,0:T(8,128)(2,1)S(1)} fusion(bf16[512,4096]{1,0:T(8,128)(2,1)} %param.33, f32[2,8,4,128]{3,2,1,0:T(4,128)S(1)} %bitcast.130, f32[2,8,4,128]{3,2,1,0:T(4,128)S(1)} %bitcast.131, f32[512]{0:T(512)S(1)} %copy-done.6), kind=kOutput, calls=%fused_computation.4 | convolution fusion | flops 67198976 | bytes 4392960 | tf_op jit(solution)/shard_map/dot_general | solution.py:122
  166.0 7.1 %all-gather = bf16[64,4096]{1,0:T(8,128)(2,1)S(1)} all-gather(bf16[16,4096]{1,0:T(8,128)(2,1)S(1)} %convolution_convert_fusion.1), channel_id=2, replica_groups=mesh['ep'=8,'tp'=4] {'tp'}, dimensions={0}, use_global_device_ids=true | all-gather | bytes 655360 | tf_op jit(solution)/shard_map/all_gather | solution.py:126
  173.9 1.8 scatter_custom_fusion
  175.7 3.6 %all-to-all-start.1 = ((bf16[8,8,4096]{2,1,0:T(8,128)(2,1)}), bf16[8,8,4096]{2,1,0:T(8,128)(2,1)S(1)}, u32[]{:S(2)}, u32[]{:S(2)}) async-start(bf16[8,8,4096]{2,1,0:T(8,128)(2,1)} %bitcast.19), calls=%async_computation.1 | async-start | bytes 1048576 | tf_op jit(solution)/shard_map/all_to_all | solution.py:144
  180.1 2.6 %broadcast_multiply_fusion = f32[16,4,128,128]{3,2,1,0:T(8,128)} fusion(f32[16,4,128]{2,1,0:T(4,128)S(1)} %bitcast.123, f32[16,4,128]{2,1,0:T(4,128)S(1)} %get-tuple-element.25), kind=kLoop, calls=%fused_computation.19 | loop fusion | flops 1048576 | bytes 4259840 | tf_op jit(solution)/shard_map/mul | solution.py:27
  182.7 5.6 %mul.268 = f32[16,4,16384]{2,1,0:T(4,128)} reshape(f32[16,4,128,128]{3,2,1,0:T(8,128)} %broadcast_multiply_fusion) | data formatting | bytes 8388608 | tf_op jit(solution)/shard_map/mul | solution.py:27
  188.3 6.0 %all-to-all-done.1 = bf16[8,8,4096]{2,1,0:T(8,128)(2,1)S(1)} async-done(((bf16[8,8,4096]{2,1,0:T(8,128)(2,1)}), bf16[8,8,4096]{2,1,0:T(8,128)(2,1)S(1)}, u32[]{:S(2)}, u32[]{:S(2)}) %all-to-all-start.1) | async-done | bytes 524320 | tf_op jit(solution)/shard_map/all_to_all | solution.py:144
  194.4 2.0 fusion.11
  196.4 3.8 %fusion = bf16[1,64,4096]{2,1,0:T(8,128)(2,1)} fusion(bf16[1,256,4096]{2,1,0:T(8,128)(2,1)S(1)} %copy-done, bf16[1,4096,256]{2,1,0:T(8,128)(2,1)} %param.39, bf16[8,8,4096]{2,1,0:T(8,128)(2,1)S(1)} %all-to-all-done.1, f32[64,256]{1,0:T(8,128)S(1)} %fusion.11), kind=kOutput, calls=%fused_computation.3 | convolution fusion | flops 268795904 | bytes 5308416 | tf_op jit(solution)/shard_map/erf,efd->erd/dot_general | solution.py:150
  200.3 6.9 %multiply_add_fusion = f32[16,4,16384]{2,1,0:T(4,128)} fusion(f32[16,4,16384]{2,1,0:T(4,128)} %mul.268, f32[16,4,16384]{2,1,0:T(4,128)} %param.30, f32[16,4]{1,0:T(8,128)S(1)} %get-tuple-element.28), kind=kLoop, calls=%fused_computation.5 | loop fusion | flops 2097152 | bytes 12583168 | tf_op jit(solution)/shard_map/add | solution.py:26
  207.9 12.5 %reduce-scatter.8.cloned.1.call-done = bf16[1,64,1024]{2,1,0:T(8,128)(2,1)} async-done(((bf16[1,64,4096]{2,1,0:T(8,128)(2,1)}), bf16[1,64,1024]{2,1,0:T(8,128)(2,1)}) %reduce-scatter.8.cloned.1.call-update) | async-done | bytes 131088 | tf_op jit(solution)/shard_map/reduce_scatter | solution.py:153
  220.4 1.1 copy.143
  222.0 1.4 reduce.1
  224.2 5.5 %all-to-all-start.2 = ((bf16[8,2,4096]{2,1,0:T(2,128)(2,1)}), bf16[8,2,4096]{2,1,0:T(2,128)(2,1)S(1)}, u32[]{:S(2)}, u32[]{:S(2)}) async-start(bf16[8,2,4096]{2,1,0:T(2,128)(2,1)} %reshape.218), calls=%async_computation.3 | async-start | bytes 262144 | tf_op jit(solution)/shard_map/all_to_all | solution.py:156
  229.7 7.3 %all-to-all-done.2 = bf16[8,2,4096]{2,1,0:T(2,128)(2,1)S(1)} async-done(((bf16[8,2,4096]{2,1,0:T(2,128)(2,1)}), bf16[8,2,4096]{2,1,0:T(2,128)(2,1)S(1)}, u32[]{:S(2)}, u32[]{:S(2)}) %all-to-all-start.2) | async-done | bytes 131104 | tf_op jit(solution)/shard_map/all_to_all | solution.py:156
  238.2 5.9 %all-reduce = (f32[16]{0:T(128)S(1)}, f32[16]{0:T(128)S(1)}) all-reduce(f32[16]{0:T(128)S(1)} %get-tuple-element.9, f32[16]{0:T(128)S(1)} %get-tuple-element.8), channel_id=1, replica_groups=mesh['ep'=8,'tp'=4] {'tp'}, use_global_device_ids=true, to_apply=%region_17.18 | all-reduce | flops 32 | bytes 256 | tf_op jit(solution)/shard_map/psum | solution.py:161
  (79 shorter events, 14.6 us)
Async XLA Ops:
  7.2 189.3 %copy-start = (bf16[1,256,4096]{2,1,0:T(8,128)(2,1)S(1)}, bf16[1,256,4096]{2,1,0:T(8,128)(2,1)}, u32[]{:S(2)}) copy-start(bf16[1,256,4096]{2,1,0:T(8,128)(2,1)} %param.40) | copy-start | bytes 6291460
  7.2 77.6 %reduce-scatter.12.cloned.1.call-start = ((), (), s32[]{:S(2)}) async-start(), calls=%async_computation.8 | async-start | bytes 73728 | tf_op jit(solution)/shard_map/reduce_scatter | solution.py:104
  24.3 3.7 %copy-start.9 = (f32[16,4]{0,1:T(4,128)S(1)}, f32[16,4]{0,1:T(4,128)}, u32[]{:S(2)}) copy-start(f32[16,4]{0,1:T(4,128)} %param.31) | copy-start | bytes 772
  24.3 127.5 %reduce-scatter.10.cloned.1.call-start = ((), (), s32[]{:S(2)}) async-start(), calls=%async_computation.7 | async-start | bytes 1179648
  28.1 6.1 %copy-start.4 = (s32[16,2]{0,1:T(2,128)S(1)}, s32[16,2]{0,1:T(2,128)}, u32[]{:S(2)}) copy-start(s32[16,2]{0,1:T(2,128)} %param.37) | copy-start | bytes 388
  28.1 56.7 %copy-start.7 = (f32[4]{0:T(128)S(1)}, f32[4]{0:T(128)}, u32[]{:S(2)}) copy-start(f32[4]{0:T(128)} %param.28) | copy-start | bytes 52
  28.1 56.7 %copy-start.8 = (f32[4]{0:T(128)S(1)}, f32[4]{0:T(128)}, u32[]{:S(2)}) copy-start(f32[4]{0:T(128)} %param.29) | copy-start | bytes 52
  85.7 76.9 %copy-start.2 = (f32[16,8]{1,0:T(8,128)S(1)}, f32[16,8]{1,0:T(8,128)}, u32[]{:S(2)}) copy-start(f32[16,8]{1,0:T(8,128)} %reduce-scatter.12.cloned.1.call-done) | copy-start | bytes 1540
  153.1 10.1 %copy-start.6 = (f32[512]{0:T(512)S(1)}, f32[512]{0:T(512)}, u32[]{:S(2)}) copy-start(f32[512]{0:T(512)} %param.32) | copy-start | bytes 6148
  162.6 10.7 %copy-start.1 = (bf16[16,4096]{1,0:T(8,128)(2,1)S(1)}, bf16[16,4096]{1,0:T(8,128)(2,1)}, u32[]{:S(2)}) copy-start(bf16[16,4096]{1,0:T(8,128)(2,1)} %param.21) | copy-start | bytes 393220
  162.6 10.9 %copy-start.3 = (f32[4096]{0:T(1024)S(1)}, f32[4096]{0:T(1024)}, u32[]{:S(2)}) copy-start(f32[4096]{0:T(1024)} %param.34) | copy-start | bytes 49156
  175.7 18.7 %all-to-all-start.1 = ((bf16[8,8,4096]{2,1,0:T(8,128)(2,1)}), bf16[8,8,4096]{2,1,0:T(8,128)(2,1)S(1)}, u32[]{:S(2)}, u32[]{:S(2)}) async-start(bf16[8,8,4096]{2,1,0:T(8,128)(2,1)} %bitcast.19), calls=%async_computation.1 | async-start | bytes 1048576 | tf_op jit(solution)/shard_map/all_to_all | solution.py:144
  179.2 41.2 %reduce-scatter.8.cloned.1.call-start = ((), (), s32[]{:S(2)}) async-start(), calls=%async_computation.6 | async-start | bytes 655360 | tf_op jit(solution)/shard_map/reduce_scatter | solution.py:153
  200.2 6.9 %copy-start.11 = (bf16[4096,2]{0,1:T(2,128)(2,1)S(1)}, bf16[4096,2]{0,1:T(2,128)(2,1)}, u32[]{:S(2)}) copy-start(bf16[4096,2]{0,1:T(2,128)(2,1)} %param.35) | copy-start | bytes 49156
  200.2 7.3 %copy-start.10 = (bf16[4096,8]{0,1:T(8,128)(2,1)S(1)}, bf16[4096,8]{0,1:T(8,128)(2,1)}, u32[]{:S(2)}) copy-start(bf16[4096,8]{0,1:T(8,128)(2,1)} %param.36) | copy-start | bytes 196612
  207.1 37.1 %copy-start.5 = (f32[1024]{0:T(1024)S(1)}, f32[1024]{0:T(1024)}, u32[]{:S(2)}) copy-start(f32[1024]{0:T(1024)} %param.41) | copy-start | bytes 12292
  224.2 12.9 %all-to-all-start.2 = ((bf16[8,2,4096]{2,1,0:T(2,128)(2,1)}), bf16[8,2,4096]{2,1,0:T(2,128)(2,1)S(1)}, u32[]{:S(2)}, u32[]{:S(2)}) async-start(bf16[8,2,4096]{2,1,0:T(2,128)(2,1)} %reshape.218), calls=%async_computation.3 | async-start | bytes 262144 | tf_op jit(solution)/shard_map/all_to_all | solution.py:156
Sparse Core Ops, SparseCore 0:
  24.4 60.3 reduce-scatter.11
  88.2 63.5 reduce-scatter.9
  200.4 20.0 reduce-scatter.7
